TPU v7x, 32 devices: a whole 2x2x4 slice. The times are simulated.
32 devices in a mesh: fs: 16 (over z, y, x), tp: 2 (over core).
Axes of the slice: x: 2, y: 2, z: 4, core: 2. Of those that a mesh axis runs over, the one named last changes fastest.
Arguments:
- tokens: bfloat16 [4096, 2048], P('fs', 'tp'), may hold values from -6 to 6
- mixer_norm_gain: bfloat16 [2048], replicated, may hold values from 0.099609375 to 1.8984375
- recurrence_branch_weight: bfloat16 [2048, 1024], P('fs', 'tp'), may hold values from -0.125 to 0.125
- output_gate_projection: bfloat16 [2048, 1024], P('fs', 'tp'), may hold values from -0.125 to 0.125
- recurrence_conv_taps: bfloat16 [4, 1024], P(None, 'tp'), may hold values from -3 to 3
- recurrence_gate_map: bfloat16 [16, 64, 64], P('tp'), may hold values from -0.75 to 0.75
- input_gate_map: bfloat16 [16, 64, 64], P('tp'), may hold values from -0.75 to 0.75
- channel_decay_rate: float32 [1024], P('tp'), may hold values from 0.001 to 0.03
- position_log_decay: float32 [4096, 1024], P('fs', 'tp'), may hold values from -0.69 to 0
- mixer_output_weight: bfloat16 [1024, 2048], P('tp', 'fs'), may hold values from -0.75 to 0.75
- feedforward_norm_gain: bfloat16 [2048], replicated, may hold values from 0.099609375 to 1.8984375
- gate_up_weight: bfloat16 [2048, 5632], P('fs', 'tp'), may hold values from -0.125 to 0.125
- value_up_weight: bfloat16 [2048, 5632], P('fs', 'tp'), may hold values from -0.125 to 0.125
- gate_conv_taps: bfloat16 [3, 5632], P(None, 'tp'), may hold values from -3 to 3
- value_conv_taps: bfloat16 [3, 5632], P(None, 'tp'), may hold values from -3 to 3
- down_projection_weight: bfloat16 [5632, 2048], P('tp', 'fs'), may hold values from -0.15625 to 0.15625
Outputs:
- result: bfloat16 [4096, 2048], P('fs', 'tp')
All inputs are finite; a program needn't handle non-finite values.
Results may differ from a plain program's by a relative error of at most 0.024.
Values may be sent and summed in bfloat16 or wider, within the bound.
A program may use at most 128 MiB of HBM per device.

v0:
```python
import jax
import jax.numpy as jnp
from jax import lax
from jax.sharding import PartitionSpec as P

SEQ_LEN = 64
EPS = 1e-06
DECAY_RATE_GAIN = 8.0


def rms_normed(values, gain):
    wide = values.astype(jnp.float32)
    factor = lax.rsqrt(jnp.mean(wide * wide, axis=-1, keepdims=True) + EPS)
    return (wide * factor * gain.astype(jnp.float32)).astype(jnp.bfloat16)


def causal_conv(values, kernel):
    width = kernel.shape[0]
    row_count, channels = values.shape
    grouped = values.astype(jnp.float32).reshape(row_count // SEQ_LEN, SEQ_LEN, channels)
    padded = jnp.pad(grouped, ((0, 0), (width - 1, 0), (0, 0)))
    summed = padded[:, 0:SEQ_LEN] * kernel[0].astype(jnp.float32)
    for offset in range(1, width):
        summed = summed + padded[:, offset : offset + SEQ_LEN] * kernel[offset].astype(jnp.float32)
    return summed.reshape(row_count, channels)


def combine(left, right):
    first_a, first_b = left
    second_a, second_b = right
    return (first_a * second_a, second_a * first_b + second_b)


def pair_folder(normed, pieces):
    return (
        jnp.dot(normed, pieces[0], preferred_element_type=jnp.float32),
        jnp.dot(normed, pieces[1], preferred_element_type=jnp.float32),
    )


def per_device(
    tokens,
    mixer_norm_gain,
    recurrence_branch_weight,
    output_gate_projection,
    recurrence_conv_taps,
    recurrence_gate_map,
    input_gate_map,
    channel_decay_rate,
    position_log_decay,
    mixer_output_weight,
    feedforward_norm_gain,
    gate_up_weight,
    value_up_weight,
    gate_conv_taps,
    value_conv_taps,
    down_projection_weight,
):
    row_count = tokens.shape[0]
    local_width = recurrence_branch_weight.shape[1]
    local_heads = recurrence_gate_map.shape[0]
    head_size = recurrence_gate_map.shape[1]
    whole_rows = lax.all_gather(tokens, "tp", axis=1, tiled=True)
    normed = rms_normed(whole_rows, mixer_norm_gain)
    branch_sum, outgate_sum = pair_folder(
        normed,
        (
            lax.all_gather(recurrence_branch_weight, "fs", axis=0, tiled=True),
            lax.all_gather(output_gate_projection, "fs", axis=0, tiled=True),
        ),
    )
    branch = branch_sum.astype(jnp.bfloat16)
    outgate = outgate_sum.astype(jnp.bfloat16)
    conv = causal_conv(branch, recurrence_conv_taps).astype(jnp.bfloat16)
    grouped = conv.reshape(row_count, local_heads, head_size)
    recurrence_scan = jax.nn.sigmoid(
        jnp.einsum(
            "rhi,hij->rhj", grouped, recurrence_gate_map, preferred_element_type=jnp.float32
        ).reshape(row_count, local_width)
    )
    inner = jax.nn.sigmoid(
        jnp.einsum(
            "rhi,hij->rhj", grouped, input_gate_map, preferred_element_type=jnp.float32
        ).reshape(row_count, local_width)
    )
    log_alpha = (
        -DECAY_RATE_GAIN * recurrence_scan * channel_decay_rate[None, :] + position_log_decay
    )
    drive = jnp.sqrt(-jnp.expm1(2.0 * log_alpha)) * inner * conv.astype(jnp.float32)
    shape3 = (row_count // SEQ_LEN, SEQ_LEN, local_width)
    unused, state = lax.associative_scan(
        combine, (jnp.exp(log_alpha).reshape(shape3), drive.reshape(shape3)), axis=1
    )
    state = state.reshape(row_count, local_width)
    mixed = (state * jax.nn.gelu(outgate.astype(jnp.float32))).astype(jnp.bfloat16)
    mixer_terms = jnp.dot(
        mixed,
        lax.all_gather(mixer_output_weight, "fs", axis=1, tiled=True),
        preferred_element_type=jnp.float32,
    )
    mixer_terms = mixer_terms.astype(jnp.bfloat16).astype(jnp.float32)
    mixer_whole = lax.psum(mixer_terms.astype(jnp.bfloat16), "tp").astype(jnp.float32)
    whole_after = (whole_rows.astype(jnp.float32) + mixer_whole).astype(jnp.bfloat16)
    normed2 = rms_normed(whole_after, feedforward_norm_gain)
    gate_whole, value_whole = (
        lax.all_gather(gate_up_weight, "fs", axis=0, tiled=True),
        lax.all_gather(value_up_weight, "fs", axis=0, tiled=True),
    )
    gate_sum = jnp.dot(normed2, gate_whole, preferred_element_type=jnp.float32)
    value_sum = jnp.dot(normed2, value_whole, preferred_element_type=jnp.float32)
    gate_half = gate_sum.astype(jnp.bfloat16)
    value_half = value_sum.astype(jnp.bfloat16)
    hidden = (
        jax.nn.silu(causal_conv(gate_half, gate_conv_taps))
        * causal_conv(value_half, value_conv_taps)
    ).astype(jnp.bfloat16)
    channel_terms = jnp.dot(
        hidden,
        lax.all_gather(down_projection_weight, "fs", axis=1, tiled=True),
        preferred_element_type=jnp.float32,
    )
    channel_terms = channel_terms.astype(jnp.bfloat16).astype(jnp.float32)
    channel_share = lax.psum_scatter(
        channel_terms.astype(jnp.bfloat16), "tp", scatter_dimension=1, tiled=True
    ).astype(jnp.float32)
    share_width = channel_share.shape[1]
    residual_share = lax.dynamic_slice_in_dim(
        whole_after, lax.axis_index("tp") * share_width, share_width, 1
    )
    return (residual_share.astype(jnp.float32) + channel_share).astype(jnp.bfloat16)


def solution(mesh):
    placed = (
        P("fs", "tp"),
        P(),
        P("fs", "tp"),
        P("fs", "tp"),
        P(None, "tp"),
        P("tp", None, None),
        P("tp", None, None),
        P("tp"),
        P("fs", "tp"),
        P("tp", "fs"),
        P(),
        P("fs", "tp"),
        P("fs", "tp"),
        P(None, "tp"),
        P(None, "tp"),
        P("tp", "fs"),
    )
    return jax.shard_map(
        per_device, mesh=mesh, in_specs=placed, out_specs=P("fs", "tp"), check_vma=False
    )
```

profile of v0, /device:TPU:0, one launch (start us, length us, event | category | flops | bytes accessed | tf_op | source)
XLA Modules:
  0.0 728.2 jit_solution(12462820517022480084)
XLA Ops:
  6.5 0.7 all-gather.8.cloned.1.call-update
  7.3 0.7 all-gather.10.cloned.1.call-update
  8.1 0.7 all-gather.12.cloned.1.call-update
  8.8 0.5 all-gather.14.cloned.1.call-update
  9.4 0.7 convert_element_type.188
  10.1 0.8 slice_convert_fusion.3
  10.9 0.7 broadcast_multiply_fusion
  11.6 9.1 %all-gather.8.cloned.1.call-done = bf16[256,2048]{1,0:T(8,128)(2,1)} async-done(((bf16[256,1024]{1,0:T(8,128)(2,1)}), bf16[256,2048]{1,0:T(8,128)(2,1)}) %all-gather.8.cloned.1.call-update) | async-done | bytes 1048592 | tf_op jit(solution)/shard_map/all_gather | solution.py:63
  20.7 1.5 fusion.15
  22.2 62.8 %all-gather.10.cloned.1.call-done = bf16[2048,512]{1,0:T(8,128)(2,1)} async-done(((bf16[128,512]{1,0:T(8,128)(2,1)}), bf16[2048,512]{1,0:T(8,128)(2,1)}) %all-gather.10.cloned.1.call-update) | async-done | bytes 2097168 | tf_op jit(solution)/shard_map/all_gather | solution.py:68
  85.0 2.7 convolution_convert_fusion.5
  87.8 0.2 fusion.30
  88.0 0.3 convert_element_type.200
  88.3 0.3 copy.22
  88.6 0.4 fusion.22
  89.0 0.2 copy.24
  89.2 0.4 fusion.24
  89.6 0.2 copy.27
  89.8 0.4 fusion.52
  90.2 0.1 slice.199
  90.4 0.1 slice.200
  90.5 0.1 slice.198
  90.7 0.1 slice.202
  91.9 0.2 slice.238
  92.1 0.2 slice.197
  93.2 0.1 pad.60
  93.5 0.1 pad.59
  93.7 53.3 %all-gather.12.cloned.1.call-done = bf16[2048,512]{1,0:T(8,128)(2,1)} async-done(((bf16[128,512]{1,0:T(8,128)(2,1)}), bf16[2048,512]{1,0:T(8,128)(2,1)}) %all-gather.12.cloned.1.call-update) | async-done | bytes 2097168 | tf_op jit(solution)/shard_map/all_gather | solution.py:69
  147.0 64.3 %all-gather.14.cloned.1.call-done = bf16[512,2048]{1,0:T(8,128)(2,1)} async-done(((bf16[512,128]{1,0:T(8,128)(2,1)}), bf16[512,2048]{1,0:T(8,128)(2,1)}) %all-gather.14.cloned.1.call-update) | async-done | bytes 2097168 | tf_op jit(solution)/shard_map/all_gather | solution.py:98
  211.3 4.7 convolution_convert_fusion.3
  216.1 0.5 all-gather.18.cloned.1.call-update
  216.7 0.7 all-gather.16.cloned.1.call-update
  217.5 0.7 all-gather.20.cloned.1.call-update
  218.2 0.2 reduce-scatter.2.cloned.1.call-start
  218.6 15.2 %all-reduce.17.cloned.1.call-done = bf16[256,2048]{1,0:T(8,128)(2,1)} async-done(((bf16[256,2048]{1,0:T(8,128)(2,1)}), bf16[256,2048]{1,0:T(8,128)(2,1)}) %all-reduce.17.cloned.1.call-update) | async-done | bytes 1048592 | tf_op jit(solution)/shard_map/psum | solution.py:102
  233.8 1.7 fusion.12
  235.6 143.5 %all-gather.18.cloned.1.call-done = bf16[2048,2816]{1,0:T(8,128)(2,1)} async-done(((bf16[128,2816]{1,0:T(8,128)(2,1)}), bf16[2048,2816]{1,0:T(8,128)(2,1)}) %all-gather.18.cloned.1.call-update) | async-done | bytes 11534352 | tf_op jit(solution)/shard_map/all_gather | solution.py:107
  379.1 7.5 %convolution_convert_fusion = bf16[256,2816]{1,0:T(8,128)(2,1)S(1)} fusion(bf16[2048,2816]{1,0:T(8,128)(2,1)} %all-gather.18.cloned.1.call-done, bf16[256,2048]{1,0:T(8,128)(2,1)S(1)} %get-tuple-element.12, f32[2048]{0:T(1024)S(1)} %convert_element_type.211, f32[256]{0:T(256)S(1)} %add_rsqrt_fusion), kind=kOutput, calls=%fused_computation | convolution fusion | flops 2955608064 | bytes 14033920 | tf_op jit(solution)/shard_map/dot_general | solution.py:110
  386.6 0.2 convert.16
  386.8 134.7 %all-gather.16.cloned.1.call-done = bf16[2048,2816]{1,0:T(8,128)(2,1)} async-done(((bf16[128,2816]{1,0:T(8,128)(2,1)}), bf16[2048,2816]{1,0:T(8,128)(2,1)}) %all-gather.16.cloned.1.call-update) | async-done | bytes 11534352 | tf_op jit(solution)/shard_map/all_gather | solution.py:106
  521.5 7.8 %convolution_convert_fusion.1 = bf16[256,2816]{1,0:T(8,128)(2,1)S(1)} fusion(bf16[2048,2816]{1,0:T(8,128)(2,1)} %all-gather.16.cloned.1.call-done, bf16[256,2048]{1,0:T(8,128)(2,1)} %copy-done.3, f32[2048]{0:T(1024)S(1)} %convert_element_type.211, f32[256]{0:T(256)S(1)} %add_rsqrt_fusion), kind=kOutput, calls=%fused_computation.1 | convolution fusion | flops 2955608064 | bytes 14033920 | tf_op jit(solution)/shard_map/dot_general | solution.py:109
  529.3 0.2 convert.15
  529.5 1.8 fusion.2
  531.3 0.8 fusion.8
  532.2 172.3 %all-gather.20.cloned.1.call-done = bf16[2816,2048]{1,0:T(8,128)(2,1)} async-done(((bf16[2816,128]{1,0:T(8,128)(2,1)}), bf16[2816,2048]{1,0:T(8,128)(2,1)}) %all-gather.20.cloned.1.call-update) | async-done | bytes 11534352 | tf_op jit(solution)/shard_map/all_gather | solution.py:119
  704.4 8.5 %convolution_convert_fusion.2 = bf16[256,2048]{1,0:T(8,128)(2,1)} fusion(bf16[256,2816]{1,0:T(8,128)(2,1)S(1)} %fusion.8, bf16[2816,2048]{1,0:T(8,128)(2,1)} %all-gather.20.cloned.1.call-done), kind=kOutput, calls=%fused_computation.26 | convolution fusion | flops 2953314304 | bytes 14024704 | tf_op jit(solution)/shard_map/dot_general | solution.py:117
  712.9 6.7 reduce-scatter.2.cloned.1.call-done
  719.7 2.0 add_convert_fusion
  (92 shorter events, 2.5 us)
Async XLA Ops:
  6.5 82.1 %copy-start = (bf16[8,64,64]{2,1,0:T(8,128)(2,1)S(1)}, bf16[8,64,64]{2,1,0:T(8,128)(2,1)}, u32[]{:S(2)}) copy-start(bf16[8,64,64]{2,1,0:T(8,128)(2,1)} %param.21) | copy-start | bytes 196612
  6.5 14.1 %all-gather.8.cloned.1.call-start = ((), (), s32[]{:S(2)}) async-start(), calls=%async_computation.1 | async-start | bytes 1572864 | tf_op jit(solution)/shard_map/all_gather | solution.py:63
  7.3 77.8 %all-gather.10.cloned.1.call-start = ((), (), s32[]{:S(2)}) async-start(), calls=%async_computation.2 | async-start | bytes 2228224 | tf_op jit(solution)/shard_map/all_gather | solution.py:68
  8.0 139.0 %all-gather.12.cloned.1.call-start = ((), (), s32[]{:S(2)}) async-start(), calls=%async_computation.3 | async-start | bytes 2228224 | tf_op jit(solution)/shard_map/all_gather | solution.py:69
  8.7 202.6 %all-gather.14.cloned.1.call-start = ((), (), s32[]{:S(2)}) async-start(), calls=%async_computation.4 | async-start | bytes 2228224 | tf_op jit(solution)/shard_map/all_gather | solution.py:98
  9.3 224.5 %all-reduce.17.cloned.1.call-start = ((), (), s32[]{:S(2)}) async-start(), calls=%async_computation.5 | async-start | bytes 2097152 | tf_op jit(solution)/shard_map/psum | solution.py:102
  87.8 1.5 copy-start.9
  88.6 1.2 copy-start.5
  93.2 118.2 %copy-start.2 = (bf16[256,2048]{1,0:T(8,128)(2,1)S(1)}, bf16[256,2048]{1,0:T(8,128)(2,1)}, u32[]{:S(2)}) copy-start(bf16[256,2048]{1,0:T(8,128)(2,1)} %all-gather.8.cloned.1.call-done) | copy-start | bytes 3145732
  216.1 2.3 copy-start.8
  216.1 2.4 copy-start.6
  216.1 2.5 copy-start.7
  216.1 163.0 %all-gather.18.cloned.1.call-start = ((), (), s32[]{:S(2)}) async-start(), calls=%async_computation.7 | async-start | bytes 12255232 | tf_op jit(solution)/shard_map/all_gather | solution.py:107
  216.7 304.8 %all-gather.16.cloned.1.call-start = ((), (), s32[]{:S(2)}) async-start(), calls=%async_computation.6 | async-start | bytes 12255232 | tf_op jit(solution)/shard_map/all_gather | solution.py:106
  217.4 487.0 %all-gather.20.cloned.1.call-start = ((), (), s32[]{:S(2)}) async-start(), calls=%async_computation.8 | async-start | bytes 12255232 | tf_op jit(solution)/shard_map/all_gather | solution.py:119
  218.2 501.5 %reduce-scatter.2.cloned.1.call-start = ((), (), s32[]{:S(2)}) async-start(), calls=%async_computation.9 | async-start | bytes 1572864 | tf_op jit(solution)/shard_map/reduce_scatter | solution.py:123
  235.6 151.0 %copy-start.3 = (bf16[256,2048]{1,0:T(8,128)(2,1)}, bf16[256,2048]{1,0:T(8,128)(2,1)S(1)}, u32[]{:S(2)}) copy-start(bf16[256,2048]{1,0:T(8,128)(2,1)S(1)} %get-tuple-element.12) | copy-start | bytes 3145732
  532.2 187.5 %copy-start.4 = (bf16[256,2048]{1,0:T(8,128)(2,1)S(1)}, bf16[256,2048]{1,0:T(8,128)(2,1)}, u32[]{:S(2)}) copy-start(bf16[256,2048]{1,0:T(8,128)(2,1)} %copy-done.3) | copy-start | bytes 3145732
  704.4 17.3 %copy-start.1 = (bf16[8,64,64]{2,1,0:T(8,128)(2,1)S(1)}, bf16[8,64,64]{2,1,0:T(8,128)(2,1)}, u32[]{:S(2)}) copy-start(bf16[8,64,64]{2,1,0:T(8,128)(2,1)} %param.21) | copy-start | bytes 196612
Sparse Core Ops, SparseCore 0:
  8.9 11.7 all-gather.7
  23.4 61.5 all-gather.9
  87.8 59.1 all-gather.11
  149.6 61.7 all-gather.13
  216.2 17.5 all-reduce.16
  236.4 142.6 all-gather.17
  381.8 139.5 all-gather.15
  524.2 180.2 all-gather.19
  713.0 6.5 reduce-scatter.1
where the time goes:
time: 729 us; the launch traced here: 728 us
  waiting for transfers between devices  666 us (91%)
  matrix products  31.8 us (4%)
  between operations  13.8 us (2%)
  other arithmetic  12.2 us (2%)
    all_gather x1, waiting for transfers between devices, per_device(): lax.all_gather(down_projection_weight, 'fs', axis=1, tiled=True)  172 us
    all_gather x1, waiting for transfers between devices, per_device(): lax.all_gather(value_up_weight, 'fs', axis=0, tiled=True)  144 us
    all_gather x1, waiting for transfers between devices, per_device(): lax.all_gather(gate_up_weight, 'fs', axis=0, tiled=True)  135 us
    all_gather x1, waiting for transfers between devices, per_device(): lax.all_gather(mixer_output_weight, 'fs', axis=1, tiled=True)  64.3 us
    all_gather x1, waiting for transfers between devices, per_device(): lax.all_gather(recurrence_branch_weight, 'fs', axis=0, tiled=True)  62.8 us
    all_gather x1, waiting for transfers between devices, per_device(): lax.all_gather(output_gate_projection, 'fs', axis=0, tiled=True)  53.3 us
    psum x1, waiting for transfers between devices, per_device(): lax.psum(mixer_terms.astype(jnp.bfloat16), 'tp').astype(jnp.float32)  15.2 us
  transfers between devices with their start and end apart: 9, of which 9 were waited for; matrix products, arithmetic and copies ran while one was open for 4% of the time, Pallas kernels for 0%

commit v1 on v0

--- a/solution.py
+++ b/solution.py
@@ -95,7 +95,12 @@
     mixed = (state * jax.nn.gelu(outgate.astype(jnp.float32))).astype(jnp.bfloat16)
     mixer_terms = jnp.dot(
         mixed,
-        lax.all_gather(mixer_output_weight, "fs", axis=1, tiled=True),
+        jnp.concatenate(
+            jax.lax.all_to_all(
+                jnp.stack([mixer_output_weight] * jax.lax.axis_size("fs"), 0), "fs", 0, 0
+            ),
+            1,
+        ),
         preferred_element_type=jnp.float32,
     )
     mixer_terms = mixer_terms.astype(jnp.bfloat16).astype(jnp.float32)

time: 729 us -> 677 us (0.929)
  waiting for transfers between devices: 666 us -> 606 us
  starting transfers between devices: 0.49 us -> 8.98 us
    all_gather x1 -> x0, waiting for transfers between devices: 64.3 us -> none  [per_device(): lax.all_gather(mixer_output_weight, 'fs', axis=1, tiled=True)]
    all_gather x1, waiting for transfers between devices: 62.8 us -> 75 us  [per_device(): lax.all_gather(recurrence_branch_weight, 'fs', axis=0, tiled=True)]
    all_to_all x0 -> x1, starting transfers between devices: none -> 8.52 us  [per_device(): jax.lax.all_to_all(jnp.stack([mixer_output_weight] * jax.lax.axis_size('f...]
    all_gather x1, waiting for transfers between devices: 9.07 us -> 0.68 us  [per_device(): whole_rows = lax.all_gather(tokens, 'tp', axis=1, tiled=True)]
  transfers between devices with their start and end apart: 9 -> 9, of which waited for: 9 -> 8; matrix products, arithmetic and copies ran while one was open for 4% -> 5% of each run, Pallas kernels for 0% -> 0%
where the time goes in v1:
time: 677 us
  waiting for transfers between devices  606 us (90%)
  matrix products  31.8 us (5%)
  between operations  14.2 us (2%)
  other arithmetic  9.97 us (1%)
  starting transfers between devices  8.98 us (1%)
    all_gather x1, waiting for transfers between devices, per_device(): lax.all_gather(down_projection_weight, 'fs', axis=1, tiled=True)  172 us
    all_gather x1, waiting for transfers between devices, per_device(): lax.all_gather(value_up_weight, 'fs', axis=0, tiled=True)  143 us
    all_gather x1, waiting for transfers between devices, per_device(): lax.all_gather(gate_up_weight, 'fs', axis=0, tiled=True)  135 us
    all_gather x1, waiting for transfers between devices, per_device(): lax.all_gather(recurrence_branch_weight, 'fs', axis=0, tiled=True)  75 us
    all_gather x1, waiting for transfers between devices, per_device(): lax.all_gather(output_gate_projection, 'fs', axis=0, tiled=True)  53 us
    psum x1, waiting for transfers between devices, per_device(): lax.psum(mixer_terms.astype(jnp.bfloat16), 'tp').astype(jnp.float32)  16 us
  transfers between devices with their start and end apart: 9, of which 8 were waited for; matrix products, arithmetic and copies ran while one was open for 5% of the time, Pallas kernels for 0%

profile of v1, /device:TPU:0, one launch (start us, length us, event | category | flops | bytes accessed | tf_op | source)
XLA Modules:
  0.0 676.8 jit_solution(4494079024308303993)
XLA Ops:
  6.5 0.7 all-gather.7.cloned.1.call-update
  7.3 0.7 all-gather.9.cloned.1.call-update
  8.0 1.0 copy.28
  9.0 1.6 stack.2
  10.6 8.5 %all-to-all-start = ((bf16[16,512,128]{1,2,0:T(8,128)(2,1)}), bf16[16,512,128]{1,2,0:T(8,128)(2,1)}, u32[]{:S(2)}, u32[]{:S(2)}) async-start(bf16[16,512,128]{1,2,0:T(8,128)(2,1)} %stack.2), calls=%async_computation | async-start | bytes 4194304 | tf_op jit(solution)/shard_map/all_to_all | solution.py:99
  19.2 0.7 all-gather.11.cloned.1.call-update
  20.0 0.7 all-gather.7.cloned.1.call-done
  20.7 1.5 fusion.15
  22.2 75.0 %all-gather.9.cloned.1.call-done = bf16[2048,512]{1,0:T(8,128)(2,1)} async-done(((bf16[128,512]{1,0:T(8,128)(2,1)}), bf16[2048,512]{1,0:T(8,128)(2,1)}) %all-gather.9.cloned.1.call-update) | async-done | bytes 2097168 | tf_op jit(solution)/shard_map/all_gather | solution.py:68
  97.2 2.7 convolution_convert_fusion.5
  99.9 0.2 fusion.30
  100.2 0.3 convert_element_type.200
  100.4 0.3 copy.22
  100.8 0.4 fusion.22
  101.2 0.2 copy.24
  101.4 0.4 fusion.24
  101.7 0.2 copy.27
  101.9 0.3 copy-done.5
  102.2 0.4 fusion.52
  102.6 0.1 slice.199
  102.8 0.1 slice.200
  103.0 0.1 slice.198
  103.1 0.1 slice.202
  104.3 0.2 slice.238
  104.5 0.2 slice.197
  105.6 0.1 pad.60
  105.9 0.1 pad.59
  106.1 53.0 %all-gather.11.cloned.1.call-done = bf16[2048,512]{1,0:T(8,128)(2,1)} async-done(((bf16[128,512]{1,0:T(8,128)(2,1)}), bf16[2048,512]{1,0:T(8,128)(2,1)}) %all-gather.11.cloned.1.call-update) | async-done | bytes 2097168 | tf_op jit(solution)/shard_map/all_gather | solution.py:69
  159.2 4.7 convolution_convert_fusion.3
  163.9 0.5 all-gather.15.cloned.1.call-update
  164.5 0.5 all-gather.13.cloned.1.call-update
  165.1 0.7 all-gather.17.cloned.1.call-update
  165.8 0.2 reduce-scatter.2.cloned.1.call-start
  166.2 0.1 convert_reduce_fusion.5
  166.3 16.0 %all-reduce.17.cloned.1.call-done = bf16[256,2048]{1,0:T(8,128)(2,1)} async-done(((bf16[256,2048]{1,0:T(8,128)(2,1)}), bf16[256,2048]{1,0:T(8,128)(2,1)}) %all-reduce.17.cloned.1.call-update) | async-done | bytes 1048592 | tf_op jit(solution)/shard_map/psum | solution.py:107
  182.3 1.7 fusion.12
  184.0 143.5 %all-gather.15.cloned.1.call-done = bf16[2048,2816]{1,0:T(8,128)(2,1)} async-done(((bf16[128,2816]{1,0:T(8,128)(2,1)}), bf16[2048,2816]{1,0:T(8,128)(2,1)}) %all-gather.15.cloned.1.call-update) | async-done | bytes 11534352 | tf_op jit(solution)/shard_map/all_gather | solution.py:112
  327.5 7.5 %convolution_convert_fusion = bf16[256,2816]{1,0:T(8,128)(2,1)S(1)} fusion(bf16[2048,2816]{1,0:T(8,128)(2,1)} %all-gather.15.cloned.1.call-done, bf16[256,2048]{1,0:T(8,128)(2,1)S(1)} %get-tuple-element.12, f32[2048]{0:T(1024)S(1)} %convert_element_type.211, f32[256]{0:T(256)S(1)} %add_rsqrt_fusion), kind=kOutput, calls=%fused_computation | convolution fusion | flops 2955608064 | bytes 14033920 | tf_op jit(solution)/shard_map/dot_general | solution.py:115
  335.0 0.2 convert.16
  335.2 134.5 %all-gather.13.cloned.1.call-done = bf16[2048,2816]{1,0:T(8,128)(2,1)} async-done(((bf16[128,2816]{1,0:T(8,128)(2,1)}), bf16[2048,2816]{1,0:T(8,128)(2,1)}) %all-gather.13.cloned.1.call-update) | async-done | bytes 11534352 | tf_op jit(solution)/shard_map/all_gather | solution.py:111
  469.8 7.8 %convolution_convert_fusion.1 = bf16[256,2816]{1,0:T(8,128)(2,1)S(1)} fusion(bf16[2048,2816]{1,0:T(8,128)(2,1)} %all-gather.13.cloned.1.call-done, bf16[256,2048]{1,0:T(8,128)(2,1)} %copy-done.3, f32[2048]{0:T(1024)S(1)} %convert_element_type.211, f32[256]{0:T(256)S(1)} %add_rsqrt_fusion), kind=kOutput, calls=%fused_computation.1 | convolution fusion | flops 2955608064 | bytes 14033920 | tf_op jit(solution)/shard_map/dot_general | solution.py:114
  477.6 0.2 convert.15
  477.8 1.8 fusion.2
  479.6 0.8 fusion.8
  480.4 172.3 %all-gather.17.cloned.1.call-done = bf16[2816,2048]{1,0:T(8,128)(2,1)} async-done(((bf16[2816,128]{1,0:T(8,128)(2,1)}), bf16[2816,2048]{1,0:T(8,128)(2,1)}) %all-gather.17.cloned.1.call-update) | async-done | bytes 11534352 | tf_op jit(solution)/shard_map/all_gather | solution.py:124
  652.7 8.5 %convolution_convert_fusion.2 = bf16[256,2048]{1,0:T(8,128)(2,1)} fusion(bf16[256,2816]{1,0:T(8,128)(2,1)S(1)} %fusion.8, bf16[2816,2048]{1,0:T(8,128)(2,1)} %all-gather.17.cloned.1.call-done), kind=kOutput, calls=%fused_computation.26 | convolution fusion | flops 2953314304 | bytes 14024704 | tf_op jit(solution)/shard_map/dot_general | solution.py:122
  661.2 6.7 reduce-scatter.2.cloned.1.call-done
  667.9 2.0 add_convert_fusion
  (99 shorter events, 2.4 us)
Async XLA Ops:
  6.5 94.2 %copy-start = (bf16[8,64,64]{2,1,0:T(8,128)(2,1)S(1)}, bf16[8,64,64]{2,1,0:T(8,128)(2,1)}, u32[]{:S(2)}) copy-start(bf16[8,64,64]{2,1,0:T(8,128)(2,1)} %param.21) | copy-start | bytes 196612
  6.5 14.1 %all-gather.7.cloned.1.call-start = ((), (), s32[]{:S(2)}) async-start(), calls=%async_computation.2 | async-start | bytes 1572864 | tf_op jit(solution)/shard_map/all_gather | solution.py:63
  7.3 89.9 %all-gather.9.cloned.1.call-start = ((), (), s32[]{:S(2)}) async-start(), calls=%async_computation.3 | async-start | bytes 2228224 | tf_op jit(solution)/shard_map/all_gather | solution.py:68
  10.6 9.3 %copy-start.9 = (bf16[2048]{0:T(1024)(128)(2,1)S(1)}, bf16[2048]{0:T(1024)(128)(2,1)}, u32[]{:S(2)}) copy-start(bf16[2048]{0:T(1024)(128)(2,1)} %param.17) | copy-start | bytes 12292
  10.6 9.3 %copy-start.8 = (bf16[4,512]{1,0:T(4,128)(2,1)S(1)}, bf16[4,512]{1,0:T(4,128)(2,1)}, u32[]{:S(2)}) copy-start(bf16[4,512]{1,0:T(4,128)(2,1)} %param.20) | copy-start | bytes 12292
  10.6 9.4 %copy-start.11 = (f32[512]{0:T(512)S(1)}, f32[512]{0:T(512)}, u32[]{:S(2)}) copy-start(f32[512]{0:T(512)} %param.23) | copy-start | bytes 6148
  10.6 95.5 %all-to-all-start = ((bf16[16,512,128]{1,2,0:T(8,128)(2,1)}), bf16[16,512,128]{1,2,0:T(8,128)(2,1)}, u32[]{:S(2)}, u32[]{:S(2)}) async-start(bf16[16,512,128]{1,2,0:T(8,128)(2,1)} %stack.2), calls=%async_computation | async-start | bytes 4194304 | tf_op jit(solution)/shard_map/all_to_all | solution.py:99
  19.1 140.0 %all-gather.11.cloned.1.call-start = ((), (), s32[]{:S(2)}) async-start(), calls=%async_computation.4 | async-start | bytes 2228224 | tf_op jit(solution)/shard_map/all_gather | solution.py:69
  19.9 162.4 %all-reduce.17.cloned.1.call-start = ((), (), s32[]{:S(2)}) async-start(), calls=%async_computation.5 | async-start | bytes 2097152 | tf_op jit(solution)/shard_map/psum | solution.py:107
  100.4 0.9 copy-start.12
  101.1 1.1 copy-start.5
  105.8 53.4 %copy-start.2 = (bf16[256,2048]{1,0:T(8,128)(2,1)S(1)}, bf16[256,2048]{1,0:T(8,128)(2,1)}, u32[]{:S(2)}) copy-start(bf16[256,2048]{1,0:T(8,128)(2,1)} %all-gather.7.cloned.1.call-done) | copy-start | bytes 3145732
  163.8 2.2 copy-start.10
  163.9 2.2 copy-start.6
  163.9 2.3 copy-start.7
  163.9 163.6 %all-gather.15.cloned.1.call-start = ((), (), s32[]{:S(2)}) async-start(), calls=%async_computation.7 | async-start | bytes 12255232 | tf_op jit(solution)/shard_map/all_gather | solution.py:112
  164.5 305.3 %all-gather.13.cloned.1.call-start = ((), (), s32[]{:S(2)}) async-start(), calls=%async_computation.6 | async-start | bytes 12255232 | tf_op jit(solution)/shard_map/all_gather | solution.py:111
  165.0 487.7 %all-gather.17.cloned.1.call-start = ((), (), s32[]{:S(2)}) async-start(), calls=%async_computation.8 | async-start | bytes 12255232 | tf_op jit(solution)/shard_map/all_gather | solution.py:124
  165.8 502.1 %reduce-scatter.2.cloned.1.call-start = ((), (), s32[]{:S(2)}) async-start(), calls=%async_computation.9 | async-start | bytes 1572864 | tf_op jit(solution)/shard_map/reduce_scatter | solution.py:128
  184.0 151.0 %copy-start.3 = (bf16[256,2048]{1,0:T(8,128)(2,1)}, bf16[256,2048]{1,0:T(8,128)(2,1)S(1)}, u32[]{:S(2)}) copy-start(bf16[256,2048]{1,0:T(8,128)(2,1)S(1)} %get-tuple-element.12) | copy-start | bytes 3145732
  480.4 187.5 %copy-start.4 = (bf16[256,2048]{1,0:T(8,128)(2,1)S(1)}, bf16[256,2048]{1,0:T(8,128)(2,1)}, u32[]{:S(2)}) copy-start(bf16[256,2048]{1,0:T(8,128)(2,1)} %copy-done.3) | copy-start | bytes 3145732
  652.7 17.2 %copy-start.1 = (bf16[8,64,64]{2,1,0:T(8,128)(2,1)S(1)}, bf16[8,64,64]{2,1,0:T(8,128)(2,1)}, u32[]{:S(2)}) copy-start(bf16[8,64,64]{2,1,0:T(8,128)(2,1)} %param.21) | copy-start | bytes 196612
Sparse Core Ops, SparseCore 0:
  8.9 11.7 all-gather.6
  23.4 73.6 all-gather.8
  99.9 59.1 all-gather.10
  164.0 18.2 all-reduce.16
  184.9 142.6 all-gather.14
  330.1 139.5 all-gather.12
  472.5 180.2 all-gather.16
  661.3 6.5 reduce-scatter.1
